TPU v7x, 32 devices: a whole 2x2x4 slice. The times are simulated.
32 devices in a mesh: dp: 2 (over x), kv: 8 (over z, y), tp: 2 (over core).
Axes of the slice: x: 2, y: 2, z: 4, core: 2. Of those that a mesh axis runs over, the one named last changes fastest.
Arguments:
- tokens: bfloat16 [48, 2048], P('dp', ('kv', 'tp')), may hold values from -21 to 21
- state: float32 [48, 8, 128, 128], P(('dp', 'kv'), 'tp'), may hold values from -3 to 3
- mix_gain: bfloat16 [2048], P(('kv', 'tp')), may hold values from 0.099609375 to 1.8984375
- w_query: bfloat16 [2048, 1024], P('kv', 'tp'), may hold values from -0.125 to 0.125
- w_key: bfloat16 [2048, 1024], P('kv', 'tp'), may hold values from -0.125 to 0.125
- w_value: bfloat16 [2048, 1024], P('kv', 'tp'), may hold values from -0.125 to 0.125
- w_beta: bfloat16 [2048, 8], P('kv', 'tp'), may hold values from -0.125 to 0.125
- w_decay: bfloat16 [2048, 8], P('kv', 'tp'), may hold values from -0.125 to 0.125
- decay_log: float32 [8], P('tp'), may hold values from -1.5 to 1
- head_gain: bfloat16 [128], replicated, may hold values from 0.099609375 to 1.8984375
- w_out: bfloat16 [1024, 2048], P('tp', 'kv'), may hold values from -0.1875 to 0.1875
- ff_gain: bfloat16 [2048], P(('kv', 'tp')), may hold values from 0.099609375 to 1.8984375
- w_up: bfloat16 [2048, 8192], P(None, ('kv', 'tp')), may hold values from -0.125 to 0.125
- w_down: bfloat16 [8192, 2048], P(('kv', 'tp')), may hold values from -0.09375 to 0.09375
Outputs:
- output: bfloat16 [48, 2048], P('dp', ('kv', 'tp'))
- new_state: float32 [48, 8, 128, 128], P(('dp', 'kv'), 'tp')
All inputs are finite; a program needn't handle non-finite values.
Results may differ from a plain program's by a relative error of at most 0.013.
Values may be sent and summed in bfloat16 or wider, within the bound.
No kernel may reach another device: no remote copies, remote signals or barrier semaphores. Data moves between devices by JAX's collectives and lax.ppermute only.
A program may use at most 64 MiB of HBM per device.

v0:
```python
import functools
import jax
import jax.numpy as jnp
from jax import lax
from jax.sharding import PartitionSpec as P

BF = jnp.bfloat16
F32 = jnp.float32


def split_pair(value):
    high = value.astype(BF)
    low = (value - lax.reduce_precision(value, 8, 7)).astype(BF)
    return (high, low)


def local(
    tokens,
    state,
    mix_gain,
    w_query,
    w_key,
    w_value,
    w_beta,
    w_decay,
    decay_log,
    head_gain,
    w_out,
    ff_gain,
    w_up,
    w_down,
    n_kv,
    n_tp,
):
    rows, width = tokens.shape
    seq, heads, size = state.shape[:3]
    n_all = n_kv * n_tp
    model = width * n_all
    keys = heads * size
    packed = jnp.concatenate([tokens, mix_gain[None, :]], axis=0)
    wide = lax.all_gather(packed, "tp", axis=1, tiled=True)
    tp_at = lax.axis_index("tp")
    out_cols = []
    for step in range(n_tp):
        target = (tp_at + step) % n_tp
        block = lax.dynamic_slice_in_dim(w_out, target * width, width, axis=1)
        if step:
            block = lax.ppermute(block, "tp", [(i, (i + step) % n_tp) for i in range(n_tp)])
        out_cols.append(block)
    wide_float = wide[:rows].astype(F32)
    scaled = (wide_float * wide[rows:].astype(F32)).astype(BF)
    dot = functools.partial(jnp.dot, preferred_element_type=F32)
    gates_part = dot(scaled, jnp.concatenate([w_beta, w_decay], axis=1))
    square_part = jnp.sum(wide_float * wide_float, axis=1, keepdims=True)
    small = jnp.concatenate([gates_part, square_part], axis=1)
    high, low = split_pair(small)
    n_small = small.shape[1]
    pad = jnp.zeros((rows, size - 2 * n_small), BF)
    sent = jnp.concatenate(
        [
            dot(scaled, w_query).astype(BF),
            dot(scaled, w_key).astype(BF),
            dot(scaled, w_value).astype(BF),
            high,
            low,
            pad,
        ],
        axis=1,
    ).reshape(n_kv, seq, 3 * keys + size)
    got = lax.all_to_all(sent, "kv", 0, 0, tiled=False)
    total = jnp.sum(got.astype(F32), axis=0)
    small = (
        total[:, 3 * keys : 3 * keys + n_small]
        + total[:, 3 * keys + n_small : 3 * keys + 2 * n_small]
    )
    inverse = lax.rsqrt(small[:, 2 * heads :] / model + 1e-06)
    query = (inverse * total[:, :keys]).reshape(seq, heads, size)
    key_rows = (inverse * total[:, keys : 2 * keys]).reshape(seq, heads, size)
    value = (inverse * total[:, 2 * keys : 3 * keys]).reshape(seq, heads, size)
    beta = jax.nn.sigmoid(inverse * small[:, :heads])
    decay = -jnp.exp(decay_log)[None, :] * jax.nn.softplus(inverse * small[:, heads : 2 * heads])
    qnorm = query * lax.rsqrt(jnp.sum(query * query, axis=-1, keepdims=True) + 1e-06)
    knorm = key_rows * lax.rsqrt(jnp.sum(key_rows * key_rows, axis=-1, keepdims=True) + 1e-06)
    kept = state * jnp.exp(decay)[:, :, None, None]
    predicted = jnp.sum(kept * knorm[:, :, :, None], axis=2)
    new_state = (
        kept + (beta[:, :, None] * knorm)[:, :, :, None] * (value - predicted)[:, :, None, :]
    )
    read = jnp.sum(new_state * qnorm[:, :, :, None], axis=2) / jnp.sqrt(jnp.float32(size))
    normed = (
        read
        * lax.rsqrt(jnp.mean(read * read, axis=-1, keepdims=True) + 1e-06)
        * head_gain.astype(F32)
    )
    normed = normed.astype(BF).reshape(seq, keys)
    axes = ("kv", "tp")
    spread = lax.all_to_all(
        jnp.broadcast_to(normed[None], (n_all, seq, keys)), axes, 0, 0, tiled=False
    )
    spread = spread.reshape(n_kv, n_tp, seq, keys)
    mixed = 0.0
    for step in range(n_tp):
        heads_of = lax.dynamic_index_in_dim(spread, (tp_at - step) % n_tp, 1, keepdims=False)
        part = dot(heads_of.reshape(rows, keys), out_cols[step])
        mixed = mixed + lax.reduce_precision(part, 8, 7)
    resid = (tokens.astype(F32) + mixed).astype(BF)
    resid_float = resid.astype(F32)
    scaled2 = (resid_float * ff_gain.astype(F32)[None, :]).astype(BF)
    high, low = split_pair(jnp.sum(resid_float * resid_float, axis=1))
    tail_rows = -(-2 * rows // width // 8) * 8
    tail = jnp.concatenate([high, low, jnp.zeros((tail_rows * width - 2 * rows,), BF)])
    tail = tail.reshape(tail_rows, width)
    sent2 = jnp.concatenate([scaled2, tail], axis=0)
    got2 = lax.all_to_all(
        jnp.broadcast_to(sent2[None], (n_all,) + sent2.shape), axes, 0, 0, tiled=False
    )
    sums = jnp.sum(
        got2[:, rows:].reshape(n_all, tail_rows * width)[:, : 2 * rows].astype(F32), axis=0
    )
    inverse2 = lax.rsqrt((sums[:rows] + sums[rows:]) / model + 1e-06)[:, None]
    whole = got2[:, :rows].transpose(1, 0, 2).reshape(rows, model)
    up_rows = dot(whole, w_up) * inverse2
    act = jnp.square(jax.nn.relu(up_rows)).astype(BF)
    down = dot(act, w_down).astype(BF).reshape(rows, n_all, width).transpose(1, 0, 2)
    got3 = lax.all_to_all(down, axes, 0, 0, tiled=False)
    output = (resid_float + jnp.sum(got3.astype(F32), axis=0)).astype(BF)
    return (output, new_state)


def solution(mesh):
    placed = (
        P("dp", ("kv", "tp")),
        P(("dp", "kv"), "tp", None, None),
        P(("kv", "tp")),
        P("kv", "tp"),
        P("kv", "tp"),
        P("kv", "tp"),
        P("kv", "tp"),
        P("kv", "tp"),
        P("tp"),
        P(),
        P("tp", "kv"),
        P(("kv", "tp")),
        P(None, ("kv", "tp")),
        P(("kv", "tp"), None),
    )
    return jax.shard_map(
        functools.partial(local, n_kv=mesh.shape["kv"], n_tp=mesh.shape["tp"]),
        mesh=mesh,
        in_specs=placed,
        out_specs=(P("dp", ("kv", "tp")), P(("dp", "kv"), "tp", None, None)),
        check_vma=False,
    )
```

profile of v0, /device:TPU:0, one launch (start us, length us, event | category | flops | bytes accessed | tf_op | source)
XLA Modules:
  0.0 61.9 jit_solution(8024021234024849064)
XLA Ops:
  0.6 0.0 copy-start
  0.6 0.0 copy-start.1
  0.7 0.9 %pad_maximum_fusion.1 = bf16[25,128]{1,0:T(8,128)(2,1)S(1)} fusion(bf16[1,128]{1,0:T(2,128)(2,1)} %bitcast.53, bf16[24,128]{1,0:T(8,128)(2,1)} %param.14), kind=kLoop, calls=%fused_computation.43 | loop fusion | flops 12800 | bytes 12800 | tf_op jit(solution)/shard_map/concatenate | solution.py:40
  1.5 2.1 %all_gather.3 = bf16[25,256]{1,0:T(8,128)(2,1)S(1)} all-gather(bf16[25,128]{1,0:T(8,128)(2,1)S(1)} %pad_maximum_fusion.1), channel_id=1, replica_groups=mesh['dp'=2,'kv'=8,'tp'=2] {'tp'}, dimensions={1}, use_global_device_ids=true | all-gather | bytes 19200 | tf_op jit(solution)/shard_map/all_gather | solution.py:41
  3.6 0.1 fusion.14
  3.8 0.1 copy.84
  3.8 0.8 %fusion.19 = f32[24,8]{1,0:T(8,128)S(1)} fusion(bf16[256,4]{0,1:T(4,128)(2,1)} %param.21, bf16[256,4]{0,1:T(4,128)(2,1)} %param.20, f32[256]{0:T(256)S(1)} %bitcast.48, bf16[25,256]{1,0:T(8,128)(2,1)S(1)} %all_gather.3), kind=kOutput, calls=%fused_computation.51 | convolution fusion | flops 124928 | bytes 18176 | tf_op jit(solution)/shard_map/dot_general | solution.py:53
  4.7 0.1 fusion.17
  4.8 0.1 fusion.23
  4.8 1.1 %convolution_convert_fusion.2 = bf16[24,512]{1,0:T(8,128)(2,1)S(1)} fusion(bf16[256,512]{1,0:T(8,128)(2,1)} %param.18, f32[256]{0:T(256)S(1)} %bitcast.49, bf16[25,256]{1,0:T(8,128)(2,1)S(1)} %all_gather.3), kind=kOutput, calls=%fused_computation.6 | convolution fusion | flops 6322176 | bytes 300032 | tf_op jit(solution)/shard_map/dot_general | solution.py:62
  5.9 0.0 copy-start.2
  5.9 1.1 %convolution_convert_fusion.1 = bf16[24,512]{1,0:T(8,128)(2,1)S(1)} fusion(bf16[256,512]{1,0:T(8,128)(2,1)} %param.19, f32[256]{0:T(256)S(1)} %bitcast.50, bf16[25,256]{1,0:T(8,128)(2,1)S(1)} %all_gather.3), kind=kOutput, calls=%fused_computation.5 | convolution fusion | flops 6322176 | bytes 300032 | tf_op jit(solution)/shard_map/dot_general | solution.py:63
  7.1 0.0 copy-start.4
  7.1 1.1 %convolution_convert_fusion.3 = bf16[24,512]{1,0:T(8,128)(2,1)S(1)} fusion(bf16[256,512]{1,0:T(8,128)(2,1)} %param.17, f32[256]{0:T(256)S(1)} %bitcast.51, bf16[25,256]{1,0:T(8,128)(2,1)S(1)} %all_gather.3), kind=kOutput, calls=%fused_computation.7 | convolution fusion | flops 6322176 | bytes 300032 | tf_op jit(solution)/shard_map/dot_general | solution.py:61
  8.2 0.1 concatenate.21
  8.3 0.0 copy-start.3
  8.3 0.7 %reshape.114 = bf16[8,3,1664]{2,1,0:T(4,128)(2,1)} reshape(bf16[24,1664]{1,0:T(8,128)(2,1)S(1)} %concatenate.21) | data formatting | bytes 159744 | tf_op jit(solution)/shard_map/reshape | solution.py:69
  9.0 7.2 %all-to-all-start = ((bf16[8,3,1664]{2,1,0:T(4,128)(2,1)}), bf16[8,3,1664]{2,1,0:T(4,128)(2,1)S(1)}, u32[]{:S(2)}, u32[]{:S(2)}) async-start(bf16[8,3,1664]{2,1,0:T(4,128)(2,1)} %reshape.114), calls=%async_computation | async-start | bytes 212992 | tf_op jit(solution)/shard_map/all_to_all | solution.py:70
  16.2 0.7 %convert_element_type.80 = f32[128]{0:T(128)S(1)} convert(bf16[128]{0:T(256)(128)(2,1)} %param.23) | non-fusion elementwise | flops 128 | bytes 768 | tf_op jit(solution)/shard_map/convert_element_type | solution.py:93
  16.8 0.7 %exponential_negate_fusion = f32[4]{0:T(128)S(1)} fusion(f32[4]{0:T(128)} %param.22), kind=kLoop, calls=%fused_computation.77 | loop fusion | flops 4 | bytes 32 | tf_op jit(solution)/shard_map/neg | solution.py:81
  17.5 5.9 %all-to-all-done = bf16[8,3,1664]{2,1,0:T(4,128)(2,1)S(1)} async-done(((bf16[8,3,1664]{2,1,0:T(4,128)(2,1)}), bf16[8,3,1664]{2,1,0:T(4,128)(2,1)S(1)}, u32[]{:S(2)}, u32[]{:S(2)}) %all-to-all-start) | async-done | bytes 79904 | tf_op jit(solution)/shard_map/all_to_all | solution.py:70
  23.3 0.1 convert_reduce_fusion
  23.4 0.1 slice_add_fusion
  23.5 0.2 rsqrt_reduce_fusion
  23.7 0.1 slice_multiply_fusion.2
  23.8 0.1 fusion.25
  23.9 0.1 multiply_reduce_fusion.5
  24.0 0.1 copy.98
  24.1 0.1 copy.86
  24.2 0.1 multiply_reduce_fusion.4
  24.3 0.1 copy.99
  24.4 0.1 copy.88
  24.5 0.1 broadcast_multiply_fusion.2
  24.6 0.0 copy-done.1
  24.6 0.3 multiply_reduce_fusion.1
  24.9 1.4 %multiply_reduce_fusion = (f32[3,4,128]{2,1,0:T(4,128)S(1)}, f32[3,4,128,128]{3,2,1,0:T(8,128)}) fusion(f32[3,4,128]{2,1,0:T(4,128)S(1)} %get-tuple-element.18, f32[3,4,128]{2,1,0:T(4,128)S(1)} %sub.17, f32[3,4,128]{2,1,0:T(4,128)S(1)} %get-tuple-element.4, f32[3,4,128,128]{3,2,1,0:T(8,128)S(1)} %copy-done.1, f32[3,4]{1,0:T(4,128)S(1)} %get-tuple-element.13), kind=kLoop, calls=%fused_computation.15 | loop fusion | flops 981504 | bytes 1597488 | tf_op jit(solution)/shard_map/reduce_sum | solution.py:89
  26.2 0.1 multiply_reduce_fusion.3
  26.3 0.1 copy.89
  26.4 0.1 copy.90
  26.5 0.1 multiply_bitcast_fusion
  26.6 0.6 %broadcast_in_dim.15 = bf16[16,3,512]{2,1,0:T(4,128)(2,1)} broadcast(bf16[3,512]{1,0:T(4,128)(2,1)S(1)} %fusion.18), dimensions={1,2} | broadcast | bytes 52224 | tf_op jit(solution)/shard_map/broadcast_in_dim | solution.py:98
  27.3 3.5 %all-to-all-start.1 = ((bf16[16,3,512]{2,1,0:T(4,128)(2,1)}), bf16[16,3,512]{2,1,0:T(4,128)(2,1)S(1)}, u32[]{:S(2)}, u32[]{:S(2)}) async-start(bf16[16,3,512]{2,1,0:T(4,128)(2,1)} %broadcast_in_dim.15), calls=%async_computation.1 | async-start | bytes 131072 | tf_op jit(solution)/shard_map/all_to_all | solution.py:97
  30.8 0.0 copy-done.2
  30.8 0.4 collective-permute-start
  31.2 0.0 copy-done.4
  31.2 6.5 %all-to-all-done.1 = bf16[16,3,512]{2,1,0:T(4,128)(2,1)S(1)} async-done(((bf16[16,3,512]{2,1,0:T(4,128)(2,1)}), bf16[16,3,512]{2,1,0:T(4,128)(2,1)S(1)}, u32[]{:S(2)}, u32[]{:S(2)}) %all-to-all-start.1) | async-done | bytes 49184 | tf_op jit(solution)/shard_map/all_to_all | solution.py:97
  37.7 0.1 convolution_reduce-precision_fusion.1
  37.9 0.0 collective-permute-done
  37.9 0.0 copy-done.3
  37.9 0.2 multiply_convert_fusion
  38.2 0.1 maximum_bitcast_fusion
  38.3 10.5 %all_to_all.20 = bf16[16,32,128]{2,1,0:T(8,128)(2,1)S(1)} all-to-all(bf16[16,32,128]{2,1,0:T(8,128)(2,1)S(1)} %broadcast_in_dim.17), channel_id=1, replica_groups=mesh['dp'=2,'kv'=8,'tp'=2] {'kv','tp'}, dimensions={0} | all-to-all | bytes 262144 | tf_op jit(solution)/shard_map/all_to_all | solution.py:114
  48.8 0.1 add_rsqrt_fusion.2
  48.9 0.0 copy-done
  48.9 2.3 %fusion = bf16[3,16,8,128]{3,2,1,0:T(8,128)(2,1)S(1)} fusion(bf16[512,2048]{1,0:T(8,128)(2,1)S(1)} %copy-done, bf16[2048,512]{1,0:T(8,128)(2,1)} %param.26, f32[24]{0:T(128)S(1)} %add_rsqrt_fusion.2, bf16[16,32,128]{2,1,0:T(8,128)(2,1)S(1)} %all_to_all.20), kind=kOutput, calls=%fused_computation.1 | convolution fusion | flops 100761600 | bytes 4391424 | tf_op jit(solution)/shard_map/dot_general | solution.py:124
  51.3 10.0 %all_to_all.21 = bf16[16,24,128]{2,1,0:T(8,128)(2,1)S(1)} all-to-all(bf16[16,24,128]{2,1,0:T(8,128)(2,1)S(1)} %bitcast.44), channel_id=1, replica_groups=mesh['dp'=2,'kv'=8,'tp'=2] {'kv','tp'}, dimensions={0} | all-to-all | bytes 196608 | tf_op jit(solution)/shard_map/all_to_all | solution.py:125
  61.3 0.6 add_convert_fusion
  (25 shorter events, 0.3 us)
Async XLA Ops:
  0.6 48.3 %copy-start = (bf16[512,2048]{1,0:T(8,128)(2,1)S(1)}, bf16[512,2048]{1,0:T(8,128)(2,1)}, u32[]{:S(2)}) copy-start(bf16[512,2048]{1,0:T(8,128)(2,1)} %param.27) | copy-start | bytes 6291460
  0.6 23.9 %copy-start.1 = (f32[3,4,128,128]{3,2,1,0:T(8,128)S(1)}, f32[3,4,128,128]{3,2,1,0:T(8,128)}, u32[]{:S(2)}) copy-start(f32[3,4,128,128]{3,2,1,0:T(8,128)} %param.15) | copy-start | bytes 2359300
  5.9 24.9 %copy-start.2 = (bf16[512,256]{1,0:T(8,128)(2,1)S(1)}, bf16[512,256]{1,0:T(8,128)(2,1)}, u32[]{:S(2)}) copy-start(bf16[512,256]{1,0:T(8,128)(2,1)} %param.24) | copy-start | bytes 786436
  7.1 24.1 %copy-start.4 = (bf16[128]{0:T(256)(128)(2,1)S(1)}, bf16[128]{0:T(256)(128)(2,1)}, u32[]{:S(2)}) copy-start(bf16[128]{0:T(256)(128)(2,1)} %param.25) | copy-start | bytes 772
  8.3 29.6 %copy-start.3 = (bf16[24,128]{1,0:T(8,128)(2,1)S(1)}, bf16[24,128]{1,0:T(8,128)(2,1)}, u32[]{:S(2)}) copy-start(bf16[24,128]{1,0:T(8,128)(2,1)} %param.14) | copy-start | bytes 18436
  9.0 14.3 %all-to-all-start = ((bf16[8,3,1664]{2,1,0:T(4,128)(2,1)}), bf16[8,3,1664]{2,1,0:T(4,128)(2,1)S(1)}, u32[]{:S(2)}, u32[]{:S(2)}) async-start(bf16[8,3,1664]{2,1,0:T(4,128)(2,1)} %reshape.114), calls=%async_computation | async-start | bytes 212992 | tf_op jit(solution)/shard_map/all_to_all | solution.py:70
  27.3 10.4 %all-to-all-start.1 = ((bf16[16,3,512]{2,1,0:T(4,128)(2,1)}), bf16[16,3,512]{2,1,0:T(4,128)(2,1)S(1)}, u32[]{:S(2)}, u32[]{:S(2)}) async-start(bf16[16,3,512]{2,1,0:T(4,128)(2,1)} %broadcast_in_dim.15), calls=%async_computation.1 | async-start | bytes 131072 | tf_op jit(solution)/shard_map/all_to_all | solution.py:97
  30.8 7.1 %collective-permute-start = (bf16[512,128]{1,0:T(8,128)(2,1)S(1)}, bf16[512,128]{1,0:T(8,128)(2,1)S(1)}, u32[]{:S(2)}, u32[]{:S(2)}) collective-permute-start(bf16[512,128]{1,0:T(8,128)(2,1)S(1)} %constant_dynamic-slice_fusion), channel_id=1, source_target_pairs={{0,1},{1,0},{2,3},{3,2},{4,5},{5,4},{6,7},{7,6},{8,9},{9,8},{10,11... | collective-permute-start | bytes 393224 | tf_op jit(solution)/shard_map/ppermute | solution.py:48
where the time goes:
time: 62.4 us; the launch traced here: 61.9 us
  blocking collectives  22.6 us (36%)
  waiting for transfers between devices  12.3 us (20%)
  starting transfers between devices  11 us (18%)
  matrix products  6.93 us (11%)
  other arithmetic  5.89 us (9%)
  local copies, waits for them, and re-layouts  2.36 us (4%)
  between operations  0.78 us (1%)
    all_to_all x1, blocking collectives, local(): lax.all_to_all(jnp.broadcast_to(sent2[None], (n_all,) + sent2.shape), axe...  10.5 us
    all_to_all x1, blocking collectives, local(): got3 = lax.all_to_all(down, axes, 0, 0, tiled=False)  9.96 us
    all_to_all x1, starting transfers between devices, local(): got = lax.all_to_all(sent, 'kv', 0, 0, tiled=False)  7.16 us
    all_to_all x1, waiting for transfers between devices, local(): lax.all_to_all(jnp.broadcast_to(normed[None], (n_all, seq, keys)), axes,...  6.46 us
    all_to_all x1, waiting for transfers between devices, local(): got = lax.all_to_all(sent, 'kv', 0, 0, tiled=False)  5.86 us
    all_to_all x1, starting transfers between devices, local(): lax.all_to_all(jnp.broadcast_to(normed[None], (n_all, seq, keys)), axes,...  3.5 us
    dot_general x1, matrix products, local(): dot(act, w_down).astype(BF).reshape(rows, n_all, width).transpose(1, 0, 2)  2.35 us
    all_gather x1, blocking collectives, local(): wide = lax.all_gather(packed, 'tp', axis=1, tiled=True)  2.11 us
  transfers between devices with their start and end apart: 3, of which 2 were waited for; matrix products, arithmetic and copies ran while one was open for 3% of the time, Pallas kernels for 0%

commit v1 on v0

--- a/solution.py
+++ b/solution.py
@@ -6,6 +6,19 @@
 
 BF = jnp.bfloat16
 F32 = jnp.float32
+
+
+def _divide_leaves(row_data, array_axis):
+    tall = jnp.concatenate(
+        lax.all_to_all(
+            jnp.stack([row_data] * lax.axis_size("tp")), axis_name="tp", split_axis=0, concat_axis=0
+        ),
+        array_axis,
+    )
+    return tall
+
+
+_wrap_frames = functools.partial(_divide_leaves, array_axis=1)
 
 
 def split_pair(value):
@@ -38,7 +51,7 @@
     model = width * n_all
     keys = heads * size
     packed = jnp.concatenate([tokens, mix_gain[None, :]], axis=0)
-    wide = lax.all_gather(packed, "tp", axis=1, tiled=True)
+    wide = _wrap_frames(packed)
     tp_at = lax.axis_index("tp")
     out_cols = []
     for step in range(n_tp):

time: 62.4 us -> 64.2 us (1.029)
  blocking collectives: 22.6 us -> 24.2 us
    all_to_all x0 -> x1, blocking collectives: none -> 3.72 us  [_divide_leaves(): lax.all_to_all(jnp.stack([row_data] * lax.axis_size('tp')), axis_name='tp...]
    all_gather x1 -> x0, blocking collectives: 2.11 us -> none  [local(): wide = lax.all_gather(packed, 'tp', axis=1, tiled=True)]
    another operation x0 -> x2, other arithmetic: none -> 0.88 us  [_divide_leaves(): jnp.stack([row_data] * lax.axis_size('tp'))]
    concatenate x1 -> x0, other arithmetic: 0.87 us -> none  [local(): packed = jnp.concatenate([tokens, mix_gain[None, :]], axis=0)]
  transfers between devices with their start and end apart: 3 -> 3, of which waited for: 2 -> 2; matrix products, arithmetic and copies ran while one was open for 3% -> 2% of each run, Pallas kernels for 0% -> 0%
where the time goes in v1:
time: 64.2 us; the launch traced here: 63.6 us
  blocking collectives  24.2 us (38%)
  waiting for transfers between devices  12.3 us (19%)
  starting transfers between devices  11.2 us (17%)
  matrix products  6.93 us (11%)
  other arithmetic  5.89 us (9%)
  local copies, waits for them, and re-layouts  2.36 us (4%)
  between operations  0.78 us (1%)
    all_to_all x1, blocking collectives, local(): lax.all_to_all(jnp.broadcast_to(sent2[None], (n_all,) + sent2.shape), axe...  10.5 us
    all_to_all x1, blocking collectives, local(): got3 = lax.all_to_all(down, axes, 0, 0, tiled=False)  9.96 us
    all_to_all x1, starting transfers between devices, local(): got = lax.all_to_all(sent, 'kv', 0, 0, tiled=False)  7.31 us
    all_to_all x1, waiting for transfers between devices, local(): lax.all_to_all(jnp.broadcast_to(normed[None], (n_all, seq, keys)), axes,...  6.46 us
    all_to_all x1, waiting for transfers between devices, local(): got = lax.all_to_all(sent, 'kv', 0, 0, tiled=False)  5.86 us
    all_to_all x1, blocking collectives, _divide_leaves(): lax.all_to_all(jnp.stack([row_data] * lax.axis_size('tp')), axis_name='tp...  3.72 us
    all_to_all x1, starting transfers between devices, local(): lax.all_to_all(jnp.broadcast_to(normed[None], (n_all, seq, keys)), axes,...  3.5 us
    dot_general x1, matrix products, local(): dot(act, w_down).astype(BF).reshape(rows, n_all, width).transpose(1, 0, 2)  2.35 us
  transfers between devices with their start and end apart: 3, of which 2 were waited for; matrix products, arithmetic and copies ran while one was open for 2% of the time, Pallas kernels for 0%

profile of v1, /device:TPU:0, one launch (start us, length us, event | category | flops | bytes accessed | tf_op | source)
XLA Modules:
  0.0 63.6 jit_solution(3839806584038207954)
XLA Ops:
  0.6 0.0 copy-start
  0.6 0.0 copy-start.1
  0.7 0.9 %maximum_bitcast_fusion = bf16[1,25,128]{2,1,0:T(8,128)(2,1)S(1)} fusion(bf16[1,128]{1,0:T(2,128)(2,1)} %bitcast.97, bf16[24,128]{1,0:T(8,128)(2,1)} %param.14), kind=kLoop, calls=%fused_computation.45 | loop fusion | flops 12800 | bytes 12800 | tf_op jit(solution)/shard_map/stack | solution.py:14
  1.5 3.7 %all_to_all.25 = bf16[2,25,128]{2,1,0:T(8,128)(2,1)S(1)} all-to-all(bf16[2,25,128]{2,1,0:T(8,128)(2,1)S(1)} %pad_maximum_fusion), channel_id=1, replica_groups=mesh['dp'=2,'kv'=8,'tp'=2] {'tp'}, dimensions={0} | all-to-all | bytes 25600 | tf_op jit(solution)/shard_map/all_to_all | solution.py:13
  5.3 0.1 fusion.13
  5.4 0.1 copy.90
  5.5 0.8 %fusion.19 = f32[24,8]{1,0:T(8,128)S(1)} fusion(bf16[256,4]{0,1:T(4,128)(2,1)} %param.21, bf16[256,4]{0,1:T(4,128)(2,1)} %param.20, f32[256]{0:T(256)S(1)} %bitcast.92, bf16[25,2,128]{2,0,1:T(8,128)(2,1)S(1)} %bitcast.85), kind=kOutput, calls=%fused_computation.53 | convolution fusion | flops 124928 | bytes 18176 | tf_op jit(solution)/shard_map/dot_general | solution.py:66
  6.3 0.1 fusion.17
  6.4 0.1 fusion.23
  6.5 1.1 %convolution_convert_fusion.2 = bf16[24,512]{1,0:T(8,128)(2,1)S(1)} fusion(bf16[256,512]{1,0:T(8,128)(2,1)} %param.18, f32[256]{0:T(256)S(1)} %bitcast.93, bf16[25,2,128]{2,0,1:T(8,128)(2,1)S(1)} %bitcast.86), kind=kOutput, calls=%fused_computation.6 | convolution fusion | flops 6322176 | bytes 300032 | tf_op jit(solution)/shard_map/dot_general | solution.py:75
  7.5 0.0 copy-start.2
  7.5 1.1 %convolution_convert_fusion.1 = bf16[24,512]{1,0:T(8,128)(2,1)S(1)} fusion(bf16[256,512]{1,0:T(8,128)(2,1)} %param.19, f32[256]{0:T(256)S(1)} %bitcast.94, bf16[25,2,128]{2,0,1:T(8,128)(2,1)S(1)} %bitcast.87), kind=kOutput, calls=%fused_computation.5 | convolution fusion | flops 6322176 | bytes 300032 | tf_op jit(solution)/shard_map/dot_general | solution.py:76
  8.7 0.0 copy-start.4
  8.7 1.1 %convolution_convert_fusion.3 = bf16[24,512]{1,0:T(8,128)(2,1)S(1)} fusion(bf16[256,512]{1,0:T(8,128)(2,1)} %param.17, f32[256]{0:T(256)S(1)} %bitcast.95, bf16[25,2,128]{2,0,1:T(8,128)(2,1)S(1)} %bitcast.88), kind=kOutput, calls=%fused_computation.7 | convolution fusion | flops 6322176 | bytes 300032 | tf_op jit(solution)/shard_map/dot_general | solution.py:74
  9.8 0.1 concatenate.21
  9.9 0.0 copy-start.3
  9.9 0.7 %reshape.132 = bf16[8,3,1664]{2,1,0:T(4,128)(2,1)} reshape(bf16[24,1664]{1,0:T(8,128)(2,1)S(1)} %concatenate.21) | data formatting | bytes 159744 | tf_op jit(solution)/shard_map/reshape | solution.py:82
  10.6 7.3 %all-to-all-start.1 = ((bf16[8,3,1664]{2,1,0:T(4,128)(2,1)}), bf16[8,3,1664]{2,1,0:T(4,128)(2,1)S(1)}, u32[]{:S(2)}, u32[]{:S(2)}) async-start(bf16[8,3,1664]{2,1,0:T(4,128)(2,1)} %reshape.132), calls=%async_computation.1 | async-start | bytes 212992 | tf_op jit(solution)/shard_map/all_to_all | solution.py:83
  17.9 0.7 %convert_element_type.100 = f32[128]{0:T(128)S(1)} convert(bf16[128]{0:T(256)(128)(2,1)} %param.23) | non-fusion elementwise | flops 128 | bytes 768 | tf_op jit(solution)/shard_map/convert_element_type | solution.py:106
  18.6 0.7 %exponential_negate_fusion = f32[4]{0:T(128)S(1)} fusion(f32[4]{0:T(128)} %param.22), kind=kLoop, calls=%fused_computation.79 | loop fusion | flops 4 | bytes 32 | tf_op jit(solution)/shard_map/neg | solution.py:94
  19.3 5.9 %all-to-all-done.1 = bf16[8,3,1664]{2,1,0:T(4,128)(2,1)S(1)} async-done(((bf16[8,3,1664]{2,1,0:T(4,128)(2,1)}), bf16[8,3,1664]{2,1,0:T(4,128)(2,1)S(1)}, u32[]{:S(2)}, u32[]{:S(2)}) %all-to-all-start.1) | async-done | bytes 79904 | tf_op jit(solution)/shard_map/all_to_all | solution.py:83
  25.1 0.1 convert_reduce_fusion
  25.2 0.1 slice_add_fusion
  25.2 0.2 rsqrt_reduce_fusion
  25.4 0.1 slice_multiply_fusion.2
  25.5 0.1 fusion.25
  25.6 0.1 multiply_reduce_fusion.5
  25.7 0.1 copy.104
  25.8 0.1 copy.92
  25.9 0.1 multiply_reduce_fusion.4
  26.0 0.1 copy.105
  26.1 0.1 copy.94
  26.2 0.1 broadcast_multiply_fusion.2
  26.3 0.0 copy-done.1
  26.3 0.3 multiply_reduce_fusion.1
  26.7 1.4 %multiply_reduce_fusion = (f32[3,4,128]{2,1,0:T(4,128)S(1)}, f32[3,4,128,128]{3,2,1,0:T(8,128)}) fusion(f32[3,4,128]{2,1,0:T(4,128)S(1)} %get-tuple-element.18, f32[3,4,128]{2,1,0:T(4,128)S(1)} %sub.17, f32[3,4,128]{2,1,0:T(4,128)S(1)} %get-tuple-element.4, f32[3,4,128,128]{3,2,1,0:T(8,128)S(1)} %copy-done.1, f32[3,4]{1,0:T(4,128)S(1)} %get-tuple-element.13), kind=kLoop, calls=%fused_computation.15 | loop fusion | flops 981504 | bytes 1597488 | tf_op jit(solution)/shard_map/reduce_sum | solution.py:102
  28.0 0.1 multiply_reduce_fusion.3
  28.1 0.1 copy.95
  28.2 0.1 copy.96
  28.3 0.1 multiply_bitcast_fusion
  28.4 0.6 %broadcast_in_dim.15 = bf16[16,3,512]{2,1,0:T(4,128)(2,1)} broadcast(bf16[3,512]{1,0:T(4,128)(2,1)S(1)} %fusion.18), dimensions={1,2} | broadcast | bytes 52224 | tf_op jit(solution)/shard_map/broadcast_in_dim | solution.py:111
  29.0 3.5 %all-to-all-start.2 = ((bf16[16,3,512]{2,1,0:T(4,128)(2,1)}), bf16[16,3,512]{2,1,0:T(4,128)(2,1)S(1)}, u32[]{:S(2)}, u32[]{:S(2)}) async-start(bf16[16,3,512]{2,1,0:T(4,128)(2,1)} %broadcast_in_dim.15), calls=%async_computation.2 | async-start | bytes 131072 | tf_op jit(solution)/shard_map/all_to_all | solution.py:110
  32.5 0.0 copy-done.2
  32.6 0.4 collective-permute-start
  32.9 0.0 copy-done.4
  32.9 6.5 %all-to-all-done.2 = bf16[16,3,512]{2,1,0:T(4,128)(2,1)S(1)} async-done(((bf16[16,3,512]{2,1,0:T(4,128)(2,1)}), bf16[16,3,512]{2,1,0:T(4,128)(2,1)S(1)}, u32[]{:S(2)}, u32[]{:S(2)}) %all-to-all-start.2) | async-done | bytes 49184 | tf_op jit(solution)/shard_map/all_to_all | solution.py:110
  39.5 0.1 convolution_reduce-precision_fusion.1
  39.6 0.0 collective-permute-done
  39.7 0.0 copy-done.3
  39.7 0.2 multiply_convert_fusion
  39.9 0.1 maximum_bitcast_fusion.1
  40.0 10.5 %all_to_all.26 = bf16[16,32,128]{2,1,0:T(8,128)(2,1)S(1)} all-to-all(bf16[16,32,128]{2,1,0:T(8,128)(2,1)S(1)} %broadcast_in_dim.17), channel_id=1, replica_groups=mesh['dp'=2,'kv'=8,'tp'=2] {'kv','tp'}, dimensions={0} | all-to-all | bytes 262144 | tf_op jit(solution)/shard_map/all_to_all | solution.py:127
  50.6 0.1 add_rsqrt_fusion.2
  50.7 0.0 copy-done
  50.7 2.3 %fusion = bf16[3,16,8,128]{3,2,1,0:T(8,128)(2,1)S(1)} fusion(bf16[512,2048]{1,0:T(8,128)(2,1)S(1)} %copy-done, bf16[2048,512]{1,0:T(8,128)(2,1)} %param.26, f32[24]{0:T(128)S(1)} %add_rsqrt_fusion.2, bf16[16,32,128]{2,1,0:T(8,128)(2,1)S(1)} %all_to_all.26), kind=kOutput, calls=%fused_computation.1 | convolution fusion | flops 100761600 | bytes 4391424 | tf_op jit(solution)/shard_map/dot_general | solution.py:137
  53.0 10.0 %all_to_all.27 = bf16[16,24,128]{2,1,0:T(8,128)(2,1)S(1)} all-to-all(bf16[16,24,128]{2,1,0:T(8,128)(2,1)S(1)} %bitcast.82), channel_id=1, replica_groups=mesh['dp'=2,'kv'=8,'tp'=2] {'kv','tp'}, dimensions={0} | all-to-all | bytes 196608 | tf_op jit(solution)/shard_map/all_to_all | solution.py:138
  63.0 0.6 add_convert_fusion
  (26 shorter events, 0.3 us)
Async XLA Ops:
  0.6 50.0 %copy-start = (bf16[512,2048]{1,0:T(8,128)(2,1)S(1)}, bf16[512,2048]{1,0:T(8,128)(2,1)}, u32[]{:S(2)}) copy-start(bf16[512,2048]{1,0:T(8,128)(2,1)} %param.27) | copy-start | bytes 6291460
  0.6 25.7 %copy-start.1 = (f32[3,4,128,128]{3,2,1,0:T(8,128)S(1)}, f32[3,4,128,128]{3,2,1,0:T(8,128)}, u32[]{:S(2)}) copy-start(f32[3,4,128,128]{3,2,1,0:T(8,128)} %param.15) | copy-start | bytes 2359300
  7.5 25.0 %copy-start.2 = (bf16[512,256]{1,0:T(8,128)(2,1)S(1)}, bf16[512,256]{1,0:T(8,128)(2,1)}, u32[]{:S(2)}) copy-start(bf16[512,256]{1,0:T(8,128)(2,1)} %param.24) | copy-start | bytes 786436
  8.7 24.2 %copy-start.4 = (bf16[128]{0:T(256)(128)(2,1)S(1)}, bf16[128]{0:T(256)(128)(2,1)}, u32[]{:S(2)}) copy-start(bf16[128]{0:T(256)(128)(2,1)} %param.25) | copy-start | bytes 772
  9.9 29.7 %copy-start.3 = (bf16[24,128]{1,0:T(8,128)(2,1)S(1)}, bf16[24,128]{1,0:T(8,128)(2,1)}, u32[]{:S(2)}) copy-start(bf16[24,128]{1,0:T(8,128)(2,1)} %param.14) | copy-start | bytes 18436
  10.6 14.5 %all-to-all-start.1 = ((bf16[8,3,1664]{2,1,0:T(4,128)(2,1)}), bf16[8,3,1664]{2,1,0:T(4,128)(2,1)S(1)}, u32[]{:S(2)}, u32[]{:S(2)}) async-start(bf16[8,3,1664]{2,1,0:T(4,128)(2,1)} %reshape.132), calls=%async_computation.1 | async-start | bytes 212992 | tf_op jit(solution)/shard_map/all_to_all | solution.py:83
  29.0 10.4 %all-to-all-start.2 = ((bf16[16,3,512]{2,1,0:T(4,128)(2,1)}), bf16[16,3,512]{2,1,0:T(4,128)(2,1)S(1)}, u32[]{:S(2)}, u32[]{:S(2)}) async-start(bf16[16,3,512]{2,1,0:T(4,128)(2,1)} %broadcast_in_dim.15), calls=%async_computation.2 | async-start | bytes 131072 | tf_op jit(solution)/shard_map/all_to_all | solution.py:110
  32.6 7.1 %collective-permute-start = (bf16[512,128]{1,0:T(8,128)(2,1)S(1)}, bf16[512,128]{1,0:T(8,128)(2,1)S(1)}, u32[]{:S(2)}, u32[]{:S(2)}) collective-permute-start(bf16[512,128]{1,0:T(8,128)(2,1)S(1)} %constant_dynamic-slice_fusion), channel_id=1, source_target_pairs={{0,1},{1,0},{2,3},{3,2},{4,5},{5,4},{6,7},{7,6},{8,9},{9,8},{10,11... | collective-permute-start | bytes 393224 | tf_op jit(solution)/shard_map/ppermute | solution.py:61
